TPU v7x, 512 devices: a whole 4x4x16 slice. The times are simulated.
512 devices in a mesh: ra: 16 (over y, x), cb: 32 (over z, core).
Axes of the slice: x: 4, y: 4, z: 16, core: 2. Of those that a mesh axis runs over, the one named last changes fastest.
Arguments:
- tokens: bfloat16 [256, 4096], P(None, 'ra'), may hold values from -20 to 20, as said below
- norm_gain: float32 [2, 4096], P(None, 'ra'), may hold values from 0.1 to 1.9
- gate_weight: bfloat16 [2, 4096, 11008], P(None, 'ra', 'cb'), may hold values from -0.09375 to 0.09375
- value_weight: bfloat16 [2, 4096, 11008], P(None, 'ra', 'cb'), may hold values from -0.09375 to 0.09375
- gate_taps: float32 [2, 3, 11008], P(None, None, 'cb'), may hold values from -3.5 to 3.5
- value_taps: float32 [2, 3, 11008], P(None, None, 'cb'), may hold values from -3.5 to 3.5
- down_weight: bfloat16 [2, 11008, 4096], P(None, 'cb', 'ra'), may hold values from -0.0546875 to 0.0546875
Outputs:
- mixed: bfloat16 [256, 4096], P(None, 'ra')
Inputs may be any that keep to these rules, and one draw needn't show every extreme that they name: tokens have features drawn around zero with a scale that varies by blocks of features between about 0.3 and 3.3.
All inputs are finite; a program needn't handle non-finite values.
Results may differ from a plain program's by a relative error of at most 0.0075.
Values may be sent and summed in bfloat16 or wider, within the bound.
A program may use at most 128 MiB of HBM per device.

v0:
```python
import jax
import jax.numpy as jnp
from jax import lax
from jax.sharding import Mesh
from jax.sharding import PartitionSpec as P

D = 4096
RA = ("ra_0", "ra_1")
epsilon = 1e-06


def laid_out(parts, dim):
    shape = list(parts.shape[1:])
    shape[dim] *= parts.shape[0]
    return jnp.moveaxis(parts, 0, dim).reshape(shape)


def copy_for_each(array, axis):
    copies = jnp.broadcast_to(array, (lax.axis_size(axis), *array.shape))
    return lax.all_to_all(copies, axis, split_axis=0, concat_axis=0, tiled=True)


def gathered_copies(array, axis, dim):
    return laid_out(copy_for_each(array, axis), dim)


def shifted(block, axis, distance):
    devices = range(lax.axis_size(axis))
    route = [(i - distance, i) for i in devices if i - distance in devices]
    return lax.ppermute(block, axis, route)


def over_pieces(array, axis):
    return lax.all_gather(array, axis).sum(0)


def split_up(array, dim, peers):
    before, after = (array.shape[:dim], array.shape[dim + 1 :])
    return jnp.moveaxis(array.reshape(*before, peers, -1, *after), dim, 0)


def moved_by_axis(parts, axes, order):
    shape = [lax.axis_size(a) for a in axes]
    parts = parts.reshape(*shape, *parts.shape[1:])
    for k in order:
        parts = lax.all_to_all(parts, axes[k], split_axis=k, concat_axis=k, tiled=True)
    return parts.reshape(-1, *parts.shape[len(axes) :])


def stepwise_exchange(array, axes, order, split_dim, concat_dim):
    parts = split_up(array, split_dim, lax.axis_size(axes))
    return laid_out(moved_by_axis(parts, axes, order), concat_dim)


def conv_after(signal, earlier, kernel_taps):
    length = signal.shape[0]
    width = kernel_taps.shape[0]
    padded = jnp.concatenate([earlier, signal], axis=0)
    result = jnp.zeros(signal.shape, jnp.float32)
    for offset in range(width):
        result = result + kernel_taps[offset] * padded[offset : offset + length]
    return result


def body(tokens, norm_gain, gate_weight, value_weight, gate_taps, value_taps, down_weight):
    stream = lax.all_to_all(tokens, RA, split_axis=0, concat_axis=1, tiled=True)
    gate_whole, value_whole, down_whole = (
        lax.all_gather(gate_weight, RA, axis=1, tiled=True),
        lax.all_gather(value_weight, RA, axis=1, tiled=True),
        lax.all_gather(down_weight, RA, axis=2, tiled=True),
    )
    gain_whole = gathered_copies(norm_gain, RA, 1)
    reach = gate_taps.shape[1] - 1
    for layer_index in range(gate_weight.shape[0]):
        current = stream.astype(jnp.float32)
        inverse_rms = lax.rsqrt(jnp.sum(current * current, axis=1, keepdims=True) / D + epsilon)
        scaled = (current * gain_whole[layer_index]).astype(jnp.bfloat16)
        gate_lin = (
            jnp.dot(scaled, gate_whole[layer_index], preferred_element_type=jnp.float32)
            * inverse_rms
        )
        value_lin = (
            jnp.dot(scaled, value_whole[layer_index], preferred_element_type=jnp.float32)
            * inverse_rms
        )
        tails = jnp.stack(
            [gate_lin[gate_lin.shape[0] - reach :], value_lin[value_lin.shape[0] - reach :]]
        )
        earlier = shifted(tails, RA, 1)
        gate_conv = conv_after(gate_lin, earlier[0], gate_taps[layer_index])
        value_conv = conv_after(value_lin, earlier[1], value_taps[layer_index])
        hidden = (jax.nn.silu(gate_conv) * value_conv).astype(jnp.bfloat16)
        partial_branch = jnp.dot(
            hidden, down_whole[layer_index], preferred_element_type=jnp.float32
        )
        branch = over_pieces(partial_branch, "cb")
        stream = (0.5 * current + branch).astype(jnp.bfloat16)
    return stepwise_exchange(stream, RA, (0, 1), 1, 0)


def solution(mesh):
    finer = Mesh(mesh.devices.reshape(4, 4, mesh.shape["cb"]), ("ra_0", "ra_1", "cb"))
    placed = (
        P(None, RA),
        P(None, RA),
        P(None, RA, "cb"),
        P(None, RA, "cb"),
        P(None, None, "cb"),
        P(None, None, "cb"),
        P(None, "cb", RA),
    )
    return jax.shard_map(body, mesh=finer, in_specs=placed, out_specs=P(None, RA), check_vma=False)
```

profile of v0, /device:TPU:32, one launch (start us, length us, event | category | flops | bytes accessed | tf_op | source)
XLA Modules:
  0.0 463.0 jit_solution(13251371283180898121)
XLA Ops:
  6.5 0.7 all-gather.8.cloned.1.call-update
  7.3 0.7 all-gather.10.cloned.1.call-update
  8.1 0.7 all-gather.12.cloned.1.call-update
  8.7 0.7 broadcast_in_dim.2
  9.4 14.4 %all_to_all.28 = f32[16,2,256]{2,1,0:T(2,128)S(1)} all-to-all(f32[16,2,256]{2,1,0:T(2,128)S(1)} %broadcast_in_dim.2), channel_id=1, replica_groups=mesh['ra_0'=4,'ra_1'=4,'cb'=32] {'ra_0','ra_1'}, dimensions={0} | all-to-all | bytes 65536 | tf_op jit(solution)/shard_map/all_to_all | solution.py:20
  23.9 3.5 all-to-all-start
  27.5 7.9 %all-to-all-done = bf16[16,16,256]{2,1,0:T(8,128)(2,1)S(1)} async-done(((bf16[16,16,256]{2,1,0:T(8,128)(2,1)}), bf16[16,16,256]{2,1,0:T(8,128)(2,1)S(1)}, u32[]{:S(2)}, u32[]{:S(2)}) %all-to-all-start) | async-done | bytes 131104 | tf_op jit(solution)/shard_map/all_to_all | solution.py:66
  35.4 0.2 fusion.10
  35.5 57.9 %all-gather.8.cloned.1.call-done = bf16[2,4096,344]{1,2,0:T(8,128)(2,1)} async-done(((bf16[2,256,344]{1,2,0:T(8,128)(2,1)}), bf16[2,4096,344]{1,2,0:T(8,128)(2,1)}) %all-gather.8.cloned.1.call-update) | async-done | bytes 5636112 | tf_op jit(solution)/shard_map/all_gather | solution.py:68
  93.5 2.6 fusion.6
  96.1 78.8 %all-gather.10.cloned.1.call-done = bf16[2,4096,344]{1,2,0:T(8,128)(2,1)} async-done(((bf16[2,256,344]{1,2,0:T(8,128)(2,1)}), bf16[2,4096,344]{1,2,0:T(8,128)(2,1)}) %all-gather.10.cloned.1.call-update) | async-done | bytes 5636112 | tf_op jit(solution)/shard_map/all_gather | solution.py:69
  174.9 2.6 fusion.7
  177.6 3.1 collective-permute-start
  180.8 1.2 collective-permute-done
  182.0 74.4 %all-gather.12.cloned.1.call-done = bf16[2,344,4096]{2,1,0:T(8,128)(2,1)} async-done(((bf16[2,344,256]{2,1,0:T(8,128)(2,1)}), bf16[2,344,4096]{2,1,0:T(8,128)(2,1)}) %all-gather.12.cloned.1.call-update) | async-done | bytes 5636112 | tf_op jit(solution)/shard_map/all_gather | solution.py:70
  256.4 3.1 fusion.3
  259.6 78.3 %all-gather.14.cloned.1.call-done = f32[512,4096]{1,0:T(8,128)} async-done(((f32[16,4096]{1,0:T(8,128)}), f32[512,4096]{1,0:T(8,128)}) %all-gather.14.cloned.1.call-update) | async-done | bytes 8388624 | tf_op jit(solution)/shard_map/all_gather | solution.py:34
  338.0 3.8 reduce_sum.41
  341.7 0.1 copy.24
  341.8 0.3 fusion.16
  342.2 2.6 fusion.8
  344.9 2.6 fusion.9
  347.5 3.3 collective-permute-start.1
  350.8 1.3 collective-permute-done.1
  352.1 3.1 fusion
  355.2 76.4 %all-gather.16.cloned.1.call-done = f32[512,4096]{1,0:T(8,128)} async-done(((f32[16,4096]{1,0:T(8,128)}), f32[512,4096]{1,0:T(8,128)}) %all-gather.16.cloned.1.call-update) | async-done | bytes 8388624 | tf_op jit(solution)/shard_map/all_gather | solution.py:34
  431.7 3.8 reduce_sum.44
  435.5 0.1 copy.26
  435.7 9.9 %all_to_all.29 = bf16[4,4,16,256]{3,1,2,0:T(4,128)(2,1)S(1)} all-to-all(bf16[4,4,16,256]{3,1,2,0:T(4,128)(2,1)S(1)} %copy.18), channel_id=1, replica_groups=mesh['ra_0'=4,'ra_1'=4,'cb'=32] {'ra_0'}, dimensions={0} | all-to-all | bytes 262144 | tf_op jit(solution)/shard_map/all_to_all | solution.py:46
  445.6 0.1 copy.19
  445.7 10.0 %all_to_all.30 = bf16[4,4,16,256]{3,0,2,1:T(4,128)(2,1)S(1)} all-to-all(bf16[4,4,16,256]{3,0,2,1:T(4,128)(2,1)S(1)} %copy.19), channel_id=1, replica_groups=mesh['ra_0'=4,'ra_1'=4,'cb'=32] {'ra_1'}, dimensions={1} | all-to-all | bytes 262144 | tf_op jit(solution)/shard_map/all_to_all | solution.py:46
  455.8 0.7 copy.20
  (31 shorter events, 0.6 us)
Async XLA Ops:
  6.5 174.2 %copy-start = (f32[2,3,344]{2,0,1:T(2,128)S(1)}, f32[2,3,344]{2,0,1:T(2,128)}, u32[]{:S(2)}) copy-start(f32[2,3,344]{2,0,1:T(2,128)} %param.12) | copy-start | bytes 24772
  6.5 174.2 %copy-start.1 = (f32[2,3,344]{2,0,1:T(2,128)S(1)}, f32[2,3,344]{2,0,1:T(2,128)}, u32[]{:S(2)}) copy-start(f32[2,3,344]{2,0,1:T(2,128)} %param.11) | copy-start | bytes 24772
  6.5 86.9 %all-gather.8.cloned.1.call-start = ((), (), s32[]{:S(2)}) async-start(), calls=%async_computation.4 | async-start | bytes 5988352 | tf_op jit(solution)/shard_map/all_gather | solution.py:68
  7.3 167.7 %all-gather.10.cloned.1.call-start = ((), (), s32[]{:S(2)}) async-start(), calls=%async_computation.5 | async-start | bytes 5988352 | tf_op jit(solution)/shard_map/all_gather | solution.py:69
  8.0 248.4 %all-gather.12.cloned.1.call-start = ((), (), s32[]{:S(2)}) async-start(), calls=%async_computation.6 | async-start | bytes 5988352 | tf_op jit(solution)/shard_map/all_gather | solution.py:70
  23.9 11.5 %all-to-all-start = ((bf16[16,16,256]{2,1,0:T(8,128)(2,1)}), bf16[16,16,256]{2,1,0:T(8,128)(2,1)S(1)}, u32[]{:S(2)}, u32[]{:S(2)}) async-start(bf16[16,16,256]{2,1,0:T(8,128)(2,1)} %bitcast.87), calls=%async_computation | async-start | bytes 262144 | tf_op jit(solution)/shard_map/all_to_all | solution.py:66
  27.4 310.6 %all-gather.14.cloned.1.call-start = ((), (), s32[]{:S(2)}) async-start(), calls=%async_computation.7 | async-start | bytes 8650752 | tf_op jit(solution)/shard_map/all_gather | solution.py:34
  177.6 4.4 collective-permute-start
  259.6 172.1 %all-gather.16.cloned.1.call-start = ((), (), s32[]{:S(2)}) async-start(), calls=%async_computation.8 | async-start | bytes 8650752 | tf_op jit(solution)/shard_map/all_gather | solution.py:34
  347.5 4.6 collective-permute-start.1
Sparse Core Ops, SparseCore 0:
  10.3 83.0 all-gather.7
  96.4 78.4 all-gather.9
  177.9 78.4 all-gather.11
  259.7 78.2 all-gather.13
  355.4 76.2 all-gather.15
where the time goes:
time: 464 us; the launch traced here: 463 us
  waiting for transfers between devices  378 us (81%)
  blocking collectives  34.4 us (7%)
  matrix products  16.7 us (4%)
  between operations  13.4 us (3%)
  starting transfers between devices  10 us (2%)
  other arithmetic  8.1 us (2%)
    all_gather x2, waiting for transfers between devices, over_pieces(): return lax.all_gather(array, axis).sum(0)  155 us
    all_gather x1, waiting for transfers between devices, body(): lax.all_gather(value_weight, RA, axis=1, tiled=True)  78.8 us
    all_gather x1, waiting for transfers between devices, body(): lax.all_gather(down_weight, RA, axis=2, tiled=True)  74.4 us
    all_gather x1, waiting for transfers between devices, body(): lax.all_gather(gate_weight, RA, axis=1, tiled=True)  57.9 us
    all_to_all x2, blocking collectives, moved_by_axis(): lax.all_to_all(parts, axes[k], split_axis=k, concat_axis=k, tiled=True)  20 us
    all_to_all x1, blocking collectives, copy_for_each(): return lax.all_to_all(copies, axis, split_axis=0, concat_axis=0, tiled=True)  14.4 us
  transfers between devices with their start and end apart: 8, of which 8 were waited for; matrix products, arithmetic and copies ran while one was open for 1% of the time, Pallas kernels for 0%

commit v1 on v0

--- a/solution.py
+++ b/solution.py
@@ -7,6 +7,13 @@
 D = 4096
 RA = ("ra_0", "ra_1")
 epsilon = 1e-06
+
+
+def define_the_sides(array_in, mesh_name):
+    local_next = jnp.stack([array_in] * lax.axis_size(mesh_name))
+    local_out = lax.all_to_all(local_next, axis_name=mesh_name, split_axis=0, concat_axis=0)
+    frame_out = jnp.concatenate(local_out, axis=2)
+    return frame_out
 
 
 def laid_out(parts, dim):
@@ -67,7 +74,7 @@
     gate_whole, value_whole, down_whole = (
         lax.all_gather(gate_weight, RA, axis=1, tiled=True),
         lax.all_gather(value_weight, RA, axis=1, tiled=True),
-        lax.all_gather(down_weight, RA, axis=2, tiled=True),
+        define_the_sides(down_weight, RA),
     )
     gain_whole = gathered_copies(norm_gain, RA, 1)
     reach = gate_taps.shape[1] - 1

time: 464 us -> 443 us (0.955)
  waiting for transfers between devices: 378 us -> 341 us
  blocking collectives: 34.4 us -> 45.9 us
  local copies, waits for them, and re-layouts: 1.91 us -> 9.41 us
    all_gather x1 -> x0, waiting for transfers between devices: 74.4 us -> none  [body(): lax.all_gather(down_weight, RA, axis=2, tiled=True)]
    all_gather x1, waiting for transfers between devices: 57.9 us -> 99.1 us  [body(): lax.all_gather(gate_weight, RA, axis=1, tiled=True)]
    all_to_all x0 -> x1, blocking collectives: none -> 11.5 us  [body(): stream = lax.all_to_all(tokens, RA, split_axis=0, concat_axis=1, tiled=True)]
    all_to_all x1, waiting for transfers between devices: 7.86 us -> 0.01 us  [define_the_sides(): lax.all_to_all(local_next, axis_name=mesh_name, split_axis=0, concat_axis=0)]
    all_gather x1, waiting for transfers between devices: 78.8 us -> 83.9 us  [body(): lax.all_gather(value_weight, RA, axis=1, tiled=True)]
  transfers between devices with their start and end apart: 8 -> 7, of which waited for: 8 -> 5; matrix products, arithmetic and copies ran while one was open for 1% -> 3% of each run, Pallas kernels for 0% -> 0%
where the time goes in v1:
time: 443 us
  waiting for transfers between devices  341 us (77%)
  blocking collectives  45.9 us (10%)
  between operations  13.4 us (3%)
  matrix products  13.1 us (3%)
  starting transfers between devices  11.2 us (3%)
  local copies, waits for them, and re-layouts  9.41 us (2%)
  other arithmetic  8.1 us (2%)
    all_gather x2, waiting for transfers between devices, over_pieces(): return lax.all_gather(array, axis).sum(0)  156 us
    all_gather x1, waiting for transfers between devices, body(): lax.all_gather(gate_weight, RA, axis=1, tiled=True)  99.1 us
    all_gather x1, waiting for transfers between devices, body(): lax.all_gather(value_weight, RA, axis=1, tiled=True)  83.9 us
    all_to_all x2, blocking collectives, moved_by_axis(): lax.all_to_all(parts, axes[k], split_axis=k, concat_axis=k, tiled=True)  20 us
    all_to_all x1, blocking collectives, copy_for_each(): return lax.all_to_all(copies, axis, split_axis=0, concat_axis=0, tiled=True)  14.4 us
    all_to_all x1, blocking collectives, body(): stream = lax.all_to_all(tokens, RA, split_axis=0, concat_axis=1, tiled=True)  11.5 us
  transfers between devices with their start and end apart: 7, of which 5 were waited for; matrix products, arithmetic and copies ran while one was open for 3% of the time, Pallas kernels for 0%

profile of v1, /device:TPU:32, one launch (start us, length us, event | category | flops | bytes accessed | tf_op | source)
XLA Modules:
  0.0 442.5 jit_solution(12750947449805139925)
XLA Ops:
  6.5 0.7 all-gather.7.cloned.1.call-update
  7.3 0.7 all-gather.9.cloned.1.call-update
  8.0 0.7 broadcast_in_dim.2
  8.7 14.4 %all_to_all.33 = f32[16,2,256]{2,1,0:T(2,128)S(1)} all-to-all(f32[16,2,256]{2,1,0:T(2,128)S(1)} %broadcast_in_dim.2), channel_id=1, replica_groups=mesh['ra_0'=4,'ra_1'=4,'cb'=32] {'ra_0','ra_1'}, dimensions={0} | all-to-all | bytes 65536 | tf_op jit(solution)/shard_map/all_to_all | solution.py:27
  23.1 11.5 %all_to_all.34 = bf16[16,16,256]{2,1,0:T(8,128)(2,1)S(1)} all-to-all(bf16[16,16,256]{2,1,0:T(8,128)(2,1)} %bitcast.96), channel_id=1, replica_groups=mesh['ra_0'=4,'ra_1'=4,'cb'=32] {'ra_0','ra_1'}, dimensions={0} | all-to-all | bytes 262144 | tf_op jit(solution)/shard_map/all_to_all | solution.py:73
  34.6 3.8 stack.17
  38.4 4.7 %all-to-all-start.2 = ((bf16[16,2,344,256]{3,2,1,0:T(8,128)(2,1)}), bf16[16,2,344,256]{3,2,1,0:T(8,128)(2,1)}, u32[]{:S(2)}, u32[]{:S(2)}) async-start(bf16[16,2,344,256]{3,2,1,0:T(8,128)(2,1)} %stack.17), calls=%async_computation.2 | async-start | bytes 11272192 | tf_op jit(solution)/shard_map/all_to_all | solution.py:14
  43.3 0.2 fusion.8
  43.5 99.1 %all-gather.7.cloned.1.call-done = bf16[2,4096,344]{1,2,0:T(8,128)(2,1)} async-done(((bf16[2,256,344]{1,2,0:T(8,128)(2,1)}), bf16[2,4096,344]{1,2,0:T(8,128)(2,1)}) %all-gather.7.cloned.1.call-update) | async-done | bytes 5636112 | tf_op jit(solution)/shard_map/all_gather | solution.py:75
  142.6 2.6 fusion.4
  145.2 83.9 %all-gather.9.cloned.1.call-done = bf16[2,4096,344]{1,2,0:T(8,128)(2,1)} async-done(((bf16[2,256,344]{1,2,0:T(8,128)(2,1)}), bf16[2,4096,344]{1,2,0:T(8,128)(2,1)}) %all-gather.9.cloned.1.call-update) | async-done | bytes 5636112 | tf_op jit(solution)/shard_map/all_gather | solution.py:76
  229.2 2.6 fusion.5
  231.9 3.1 collective-permute-start
  235.0 3.0 fusion.64
  238.0 0.3 copy.28
  238.4 1.3 fusion.41
  239.8 79.6 %all-gather.11.cloned.1.call-done = f32[512,4096]{1,0:T(8,128)} async-done(((f32[16,4096]{1,0:T(8,128)}), f32[512,4096]{1,0:T(8,128)}) %all-gather.11.cloned.1.call-update) | async-done | bytes 8388624 | tf_op jit(solution)/shard_map/all_gather | solution.py:41
  319.3 3.8 reduce_sum.41
  323.2 0.3 fusion.14
  323.6 2.6 fusion.6
  326.2 2.6 fusion.7
  328.9 3.3 collective-permute-start.1
  332.2 0.3 copy.31
  332.5 1.0 collective-permute-done.1
  333.5 1.3 fusion.43
  334.8 76.4 %all-gather.13.cloned.1.call-done = f32[512,4096]{1,0:T(8,128)} async-done(((f32[16,4096]{1,0:T(8,128)}), f32[512,4096]{1,0:T(8,128)}) %all-gather.13.cloned.1.call-update) | async-done | bytes 8388624 | tf_op jit(solution)/shard_map/all_gather | solution.py:41
  411.2 3.8 reduce_sum.44
  415.0 0.1 copy.32
  415.3 9.9 %all_to_all.35 = bf16[4,4,16,256]{3,1,2,0:T(4,128)(2,1)S(1)} all-to-all(bf16[4,4,16,256]{3,1,2,0:T(4,128)(2,1)S(1)} %copy.22), channel_id=1, replica_groups=mesh['ra_0'=4,'ra_1'=4,'cb'=32] {'ra_0'}, dimensions={0} | all-to-all | bytes 262144 | tf_op jit(solution)/shard_map/all_to_all | solution.py:53
  425.2 0.1 copy.23
  425.3 10.0 %all_to_all.36 = bf16[4,4,16,256]{3,0,2,1:T(4,128)(2,1)S(1)} all-to-all(bf16[4,4,16,256]{3,0,2,1:T(4,128)(2,1)S(1)} %copy.23), channel_id=1, replica_groups=mesh['ra_0'=4,'ra_1'=4,'cb'=32] {'ra_1'}, dimensions={1} | all-to-all | bytes 262144 | tf_op jit(solution)/shard_map/all_to_all | solution.py:53
  435.3 0.7 copy.24
  (33 shorter events, 0.6 us)
Async XLA Ops:
  6.5 136.0 %all-gather.7.cloned.1.call-start = ((), (), s32[]{:S(2)}) async-start(), calls=%async_computation.5 | async-start | bytes 5988352 | tf_op jit(solution)/shard_map/all_gather | solution.py:75
  7.3 221.9 %all-gather.9.cloned.1.call-start = ((), (), s32[]{:S(2)}) async-start(), calls=%async_computation.6 | async-start | bytes 5988352 | tf_op jit(solution)/shard_map/all_gather | solution.py:76
  38.4 4.8 %copy-start = (f32[2,3,344]{2,0,1:T(2,128)S(1)}, f32[2,3,344]{2,0,1:T(2,128)}, u32[]{:S(2)}) copy-start(f32[2,3,344]{2,0,1:T(2,128)} %param.12) | copy-start | bytes 24772
  38.4 4.8 %copy-start.1 = (f32[2,3,344]{2,0,1:T(2,128)S(1)}, f32[2,3,344]{2,0,1:T(2,128)}, u32[]{:S(2)}) copy-start(f32[2,3,344]{2,0,1:T(2,128)} %param.11) | copy-start | bytes 24772
  38.4 196.6 %all-to-all-start.2 = ((bf16[16,2,344,256]{3,2,1,0:T(8,128)(2,1)}), bf16[16,2,344,256]{3,2,1,0:T(8,128)(2,1)}, u32[]{:S(2)}, u32[]{:S(2)}) async-start(bf16[16,2,344,256]{3,2,1,0:T(8,128)(2,1)} %stack.17), calls=%async_computation.2 | async-start | bytes 11272192 | tf_op jit(solution)/shard_map/all_to_all | solution.py:14
  43.1 276.2 %all-gather.11.cloned.1.call-start = ((), (), s32[]{:S(2)}) async-start(), calls=%async_computation.7 | async-start | bytes 8650752 | tf_op jit(solution)/shard_map/all_gather | solution.py:41
  231.9 6.5 %collective-permute-start = (f32[2,2,344]{2,1,0:T(2,128)S(1)}, f32[2,2,344]{2,1,0:T(2,128)S(1)}, u32[]{:S(2)}, u32[]{:S(2)}) collective-permute-start(f32[2,2,344]{2,1,0:T(2,128)S(1)} %pad_maximum_fusion.4), channel_id=1, source_target_pairs={{0,32},{32,64},{64,96},{96,128},{128,160},{160,192},{192,224},{224... | collective-permute-start | bytes 16520 | tf_op jit(solution)/shard_map/ppermute | solution.py:37
  239.7 171.6 %all-gather.13.cloned.1.call-start = ((), (), s32[]{:S(2)}) async-start(), calls=%async_computation.8 | async-start | bytes 8650752 | tf_op jit(solution)/shard_map/all_gather | solution.py:41
  328.9 4.6 %collective-permute-start.1 = (f32[2,2,344]{2,1,0:T(2,128)S(1)}, f32[2,2,344]{2,1,0:T(2,128)S(1)}, u32[]{:S(2)}, u32[]{:S(2)}) collective-permute-start(f32[2,2,344]{2,1,0:T(2,128)S(1)} %pad_maximum_fusion.5), channel_id=1, source_target_pairs={{0,32},{32,64},{64,96},{96,128},{128,160},{160,192},{192,224},{224... | collective-permute-start | bytes 16520 | tf_op jit(solution)/shard_map/ppermute | solution.py:37
Sparse Core Ops, SparseCore 0:
  10.3 132.2 all-gather.6
  145.6 83.5 all-gather.8
  239.8 79.4 all-gather.10
  334.9 76.2 all-gather.12
